TPU v7x, 32 devices: a whole 2x2x4 slice. The times are simulated.
32 devices in a mesh: ra: 4 (over z), cb: 4 (over y, x), dp: 2 (over core).
Axes of the slice: x: 2, y: 2, z: 4, core: 2. Of those that a mesh axis runs over, the one named last changes fastest.
Arguments:
- tokens: bfloat16 [256, 4096], P('dp', 'ra'), may hold values from -24 to 24
- first_gain: float32 [4096], P('ra'), may hold values from 0.1 to 1.9
- first_gate: float32 [4096, 11264], P('ra', 'cb'), may hold values from -0.125 to 0.125
- first_gate_scale: float32 [11264], P('cb'), may hold values from 0.5 to 2
- first_up: float32 [4096, 11264], P('ra', 'cb'), may hold values from -0.125 to 0.125
- first_up_scale: float32 [11264], P('cb'), may hold values from 0.5 to 2
- first_down: float32 [11264, 4096], P('cb', 'ra'), may hold values from -0.0546875 to 0.0546875
- first_down_scale: float32 [4096], P('ra'), may hold values from 0.5 to 2
- second_gain: float32 [4096], P('ra'), may hold values from 0.1 to 1.9
- second_gate: float32 [4096, 11264], P('ra', 'cb'), may hold values from -0.125 to 0.125
- second_gate_scale: float32 [11264], P('cb'), may hold values from 0.5 to 2
- second_up: float32 [4096, 11264], P('ra', 'cb'), may hold values from -0.125 to 0.125
- second_up_scale: float32 [11264], P('cb'), may hold values from 0.5 to 2
- second_down: float32 [11264, 4096], P('cb', 'ra'), may hold values from -0.0546875 to 0.0546875
- second_down_scale: float32 [4096], P('ra'), may hold values from 0.5 to 2
Outputs:
- mixed: float32 [256, 4096], P('dp', 'ra')
All inputs are finite; a program needn't handle non-finite values.
Results may differ from a plain program's by a relative error of at most 0.0083.
Values may be sent and summed in bfloat16 or wider, within the bound.
A program may use at most 128 MiB of HBM per device.

v0:
```python
import jax
import jax.numpy as jnp
from jax import lax
from jax.sharding import PartitionSpec as P


def half_step(stream, gain, gate_w, gate_scale, up_w, up_scale, down_w, down_scale):
    squares = jnp.sum(stream * stream, axis=1)
    width = stream.shape[1] * lax.axis_size("ra")
    scaled = (stream * gain).astype(jnp.bfloat16)
    gate_part = jnp.dot(scaled, gate_w.astype(jnp.bfloat16), preferred_element_type=jnp.float32)
    up_part = jnp.dot(scaled, up_w.astype(jnp.bfloat16), preferred_element_type=jnp.float32)
    down_bf = down_w.astype(jnp.bfloat16)
    total = lax.psum(squares, "ra")
    inverse = lax.rsqrt(total / width + 1e-06)[:, None]
    gate_sum, up_sum = (
        lax.psum_scatter(gate_part, "ra", scatter_dimension=1, tiled=True),
        lax.psum_scatter(up_part, "ra", scatter_dimension=1, tiled=True),
    )
    columns = gate_sum.shape[1]
    offset = lax.axis_index("ra") * columns
    gate_own = lax.dynamic_slice_in_dim(gate_scale, offset, columns, 0)
    up_own = lax.dynamic_slice_in_dim(up_scale, offset, columns, 0)
    hidden = (jax.nn.silu(gate_sum * inverse * gate_own) * (up_sum * inverse * up_own)).astype(
        jnp.bfloat16
    )
    partial_value = jnp.dot(
        lax.all_gather(hidden, "ra", axis=1, tiled=True),
        down_bf,
        preferred_element_type=jnp.float32,
    )
    branch = lax.psum(partial_value, "cb")
    return 0.5 * stream + 0.5 * branch * down_scale


def local(
    tokens,
    first_gain,
    first_gate,
    first_gate_scale,
    first_up,
    first_up_scale,
    first_down,
    first_down_scale,
    second_gain,
    second_gate,
    second_gate_scale,
    second_up,
    second_up_scale,
    second_down,
    second_down_scale,
):
    stream = tokens.astype(jnp.float32)
    stream = half_step(
        stream,
        first_gain,
        first_gate,
        first_gate_scale,
        first_up,
        first_up_scale,
        first_down,
        first_down_scale,
    )
    stream = half_step(
        stream,
        second_gain,
        second_gate,
        second_gate_scale,
        second_up,
        second_up_scale,
        second_down,
        second_down_scale,
    )
    return stream


def solution(mesh):
    placed = (
        P("dp", "ra"),
        P("ra"),
        P("ra", "cb"),
        P("cb"),
        P("ra", "cb"),
        P("cb"),
        P("cb", "ra"),
        P("ra"),
        P("ra"),
        P("ra", "cb"),
        P("cb"),
        P("ra", "cb"),
        P("cb"),
        P("cb", "ra"),
        P("ra"),
    )
    return jax.shard_map(
        local, mesh=mesh, in_specs=placed, out_specs=P("dp", "ra"), check_vma=False
    )
```

profile of v0, /device:TPU:0, one launch (start us, length us, event | category | flops | bytes accessed | tf_op | source)
XLA Modules:
  0.0 308.8 jit_solution(2525451048943693273)
XLA Ops:
  6.5 0.0 copy-start
  6.5 0.0 copy-start.2
  6.5 0.0 reduce-scatter.5.cloned.1.call-start
  6.5 7.9 %fusion.10 = f32[128,2816]{0,1:T(8,128)} fusion(f32[1024,2816]{1,0:T(8,128)} %param.17, bf16[128,1024]{1,0:T(8,128)(2,1)} %param.15, f32[1024]{0:T(1024)} %param.16), kind=kOutput, calls=%fused_computation.10 | convolution fusion | flops 741474304 | bytes 13242368 | tf_op jit(solution)/shard_map/dot_general | solution.py:11
  14.4 0.0 reduce-scatter.5.cloned.1.call-update
  14.5 0.0 reduce-scatter.7.cloned.1.call-start
  14.5 0.0 copy-done
  14.5 0.0 copy-done.2
  14.5 7.7 %fusion.8 = f32[128,2816]{0,1:T(8,128)} fusion(f32[1024,2816]{1,0:T(8,128)} %param.19, bf16[128,1024]{1,0:T(8,128)(2,1)S(1)} %copy-done, f32[1024]{0:T(1024)S(1)} %copy-done.2), kind=kOutput, calls=%fused_computation.8 | convolution fusion | flops 741474304 | bytes 13242368 | tf_op jit(solution)/shard_map/dot_general | solution.py:12
  22.3 0.0 reduce-scatter.7.cloned.1.call-update
  22.3 0.0 all-reduce.3.cloned.1.call-start
  22.4 0.8 dynamic_slice.12
  23.1 0.8 dynamic_slice.13
  23.9 0.1 fusion.14
  24.0 13.9 %psum.28 = f32[128]{0:T(128)S(1)} all-reduce(f32[128]{0:T(128)S(1)} %fusion.14), channel_id=1, replica_groups=mesh['ra'=4,'cb'=4,'dp'=2] {'ra'}, use_global_device_ids=true, to_apply=%region_2.0 | all-reduce | flops 128 | bytes 1024 | tf_op jit(solution)/shard_map/psum | solution.py:14
  38.0 13.0 %reduce-scatter.5.cloned.1.call-done = f32[128,704]{0,1:T(8,128)} async-done(((f32[128,2816]{0,1:T(8,128)}), f32[128,704]{0,1:T(8,128)}) %reduce-scatter.5.cloned.1.call-update) | async-done | bytes 360464 | tf_op jit(solution)/shard_map/reduce_scatter | solution.py:17
  51.0 34.5 %reduce-scatter.7.cloned.1.call-done = f32[128,704]{0,1:T(8,128)} async-done(((f32[128,2816]{0,1:T(8,128)}), f32[128,704]{0,1:T(8,128)}) %reduce-scatter.7.cloned.1.call-update) | async-done | bytes 360464 | tf_op jit(solution)/shard_map/reduce_scatter | solution.py:18
  85.5 1.3 multiply_convert_fusion.2
  86.9 17.2 %all_gather.6 = bf16[128,2816]{0,1:T(8,128)(2,1)S(1)} all-gather(bf16[128,704]{0,1:T(8,128)(2,1)S(1)} %multiply_convert_fusion.2), channel_id=1, replica_groups=mesh['ra'=4,'cb'=4,'dp'=2] {'ra'}, dimensions={1}, use_global_device_ids=true | all-gather | bytes 901120 | tf_op jit(solution)/shard_map/all_gather | solution.py:28
  104.1 0.0 copy-start.4
  104.1 0.0 copy-start.3
  104.1 6.0 %fusion.6 = f32[128,1024]{1,0:T(8,128)} fusion(bf16[128,2816]{0,1:T(8,128)(2,1)S(1)} %all_gather.6, f32[2816,1024]{1,0:T(8,128)} %param.21), kind=kOutput, calls=%fused_computation.6 | convolution fusion | flops 741081088 | bytes 12779520 | tf_op jit(solution)/shard_map/dot_general | solution.py:27
  110.1 0.0 all-reduce.3.cloned.1.call-update
  110.1 0.0 reduce-scatter.11.cloned.1.call-start
  110.2 0.0 copy-done.4
  110.2 44.4 %all-reduce.3.cloned.1.call-done = f32[128,1024]{1,0:T(8,128)} async-done(((f32[128,1024]{1,0:T(8,128)}), f32[128,1024]{1,0:T(8,128)}) %all-reduce.3.cloned.1.call-update) | async-done | bytes 524304 | tf_op jit(solution)/shard_map/psum | solution.py:32
  154.6 0.0 copy-done.3
  154.6 0.0 copy-start.1
  154.6 8.0 %fusion.2 = f32[128,2816]{0,1:T(8,128)} fusion(f32[1024,2816]{1,0:T(8,128)} %param.26, f32[1024]{0:T(1024)S(1)} %copy-done.3, bf16[128,1024]{1,0:T(8,128)(2,1)S(1)} %copy-done, f32[128,1024]{1,0:T(8,128)} %all-reduce.3.cloned.1.call-done, f32[1024]{0:T(1024)S(1)} %broadcast_multiply_fusion.1), kind=kOutput, calls=%fused_computation.2 | convolution fusion | flops 741867520 | bytes 13770752 | tf_op jit(solution)/shard_map/dot_general | solution.py:12
  162.6 0.0 reduce-scatter.11.cloned.1.call-update
  162.6 0.0 reduce-scatter.9.cloned.1.call-start
  162.7 0.0 copy-done.1
  162.7 7.7 %fusion.4 = f32[128,2816]{0,1:T(8,128)} fusion(f32[1024,2816]{1,0:T(8,128)} %param.24, f32[1024]{0:T(1024)S(1)} %copy-done.3, bf16[128,1024]{1,0:T(8,128)(2,1)S(1)} %copy-done, f32[128,1024]{1,0:T(8,128)S(1)} %copy-done.1, f32[1024]{0:T(1024)S(1)} %broadcast_multiply_fusion.1), kind=kOutput, calls=%fused_computation.4 | convolution fusion | flops 741867520 | bytes 13770752 | tf_op jit(solution)/shard_map/dot_general | solution.py:11
  170.4 0.0 reduce-scatter.9.cloned.1.call-update
  170.4 0.0 all-reduce.5.cloned.1.call-start
  170.5 0.8 dynamic_slice.14
  171.3 0.8 dynamic_slice.15
  172.0 0.2 multiply_reduce_fusion
  172.2 12.2 %psum.30 = f32[128]{0:T(128)S(1)} all-reduce(f32[128]{0:T(128)S(1)} %multiply_reduce_fusion), channel_id=1, replica_groups=mesh['ra'=4,'cb'=4,'dp'=2] {'ra'}, use_global_device_ids=true, to_apply=%region_7.8 | all-reduce | flops 128 | bytes 1024 | tf_op jit(solution)/shard_map/psum | solution.py:14
  184.5 12.0 %reduce-scatter.11.cloned.1.call-done = f32[128,704]{0,1:T(8,128)} async-done(((f32[128,2816]{0,1:T(8,128)}), f32[128,704]{0,1:T(8,128)}) %reduce-scatter.11.cloned.1.call-update) | async-done | bytes 360464 | tf_op jit(solution)/shard_map/reduce_scatter | solution.py:18
  196.4 34.4 %reduce-scatter.9.cloned.1.call-done = f32[128,704]{0,1:T(8,128)} async-done(((f32[128,2816]{0,1:T(8,128)}), f32[128,704]{0,1:T(8,128)}) %reduce-scatter.9.cloned.1.call-update) | async-done | bytes 360464 | tf_op jit(solution)/shard_map/reduce_scatter | solution.py:17
  230.8 1.3 multiply_convert_fusion.1
  232.2 17.2 %all_gather.7 = bf16[128,2816]{0,1:T(8,128)(2,1)S(1)} all-gather(bf16[128,704]{0,1:T(8,128)(2,1)S(1)} %multiply_convert_fusion.1), channel_id=1, replica_groups=mesh['ra'=4,'cb'=4,'dp'=2] {'ra'}, dimensions={1}, use_global_device_ids=true | all-gather | bytes 901120 | tf_op jit(solution)/shard_map/all_gather | solution.py:28
  249.4 0.0 copy-start.5
  249.4 6.0 %fusion = f32[128,1024]{1,0:T(8,128)} fusion(bf16[128,2816]{0,1:T(8,128)(2,1)S(1)} %all_gather.7, f32[2816,1024]{1,0:T(8,128)} %param.28), kind=kOutput, calls=%fused_computation | convolution fusion | flops 741081088 | bytes 12779520 | tf_op jit(solution)/shard_map/dot_general | solution.py:27
  255.4 0.0 all-reduce.5.cloned.1.call-update
  255.4 0.0 copy-done.5
  255.5 44.5 %all-reduce.5.cloned.1.call-done = f32[128,1024]{1,0:T(8,128)} async-done(((f32[128,1024]{1,0:T(8,128)}), f32[128,1024]{1,0:T(8,128)}) %all-reduce.5.cloned.1.call-update) | async-done | bytes 524304 | tf_op jit(solution)/shard_map/psum | solution.py:32
  299.9 2.0 multiply_add_fusion
  (4 shorter events, 0.0 us)
Async XLA Ops:
  6.5 8.0 %copy-start = (bf16[128,1024]{1,0:T(8,128)(2,1)S(1)}, bf16[128,1024]{1,0:T(8,128)(2,1)}, u32[]{:S(2)}) copy-start(bf16[128,1024]{1,0:T(8,128)(2,1)} %param.15) | copy-start | bytes 786436
  6.5 8.0 %copy-start.2 = (f32[1024]{0:T(1024)S(1)}, f32[1024]{0:T(1024)}, u32[]{:S(2)}) copy-start(f32[1024]{0:T(1024)} %param.16) | copy-start | bytes 12292
  6.5 44.5 %reduce-scatter.5.cloned.1.call-start = ((), (), s32[]{:S(2)}) async-start(), calls=%async_computation.4 | async-start | bytes 1802240 | tf_op jit(solution)/shard_map/reduce_scatter | solution.py:17
  14.5 71.1 %reduce-scatter.7.cloned.1.call-start = ((), (), s32[]{:S(2)}) async-start(), calls=%async_computation.5 | async-start | bytes 1802240 | tf_op jit(solution)/shard_map/reduce_scatter | solution.py:18
  22.3 132.3 %all-reduce.3.cloned.1.call-start = ((), (), s32[]{:S(2)}) async-start(), calls=%async_computation.6 | async-start | bytes 1048576 | tf_op jit(solution)/shard_map/psum | solution.py:32
  104.1 6.1 %copy-start.4 = (f32[1024]{0:T(1024)S(1)}, f32[1024]{0:T(1024)}, u32[]{:S(2)}) copy-start(f32[1024]{0:T(1024)} %param.22) | copy-start | bytes 12292
  104.1 50.6 %copy-start.3 = (f32[1024]{0:T(1024)S(1)}, f32[1024]{0:T(1024)}, u32[]{:S(2)}) copy-start(f32[1024]{0:T(1024)} %param.23) | copy-start | bytes 12292
  110.1 86.3 %reduce-scatter.11.cloned.1.call-start = ((), (), s32[]{:S(2)}) async-start(), calls=%async_computation.8 | async-start | bytes 1802240 | tf_op jit(solution)/shard_map/reduce_scatter | solution.py:18
  154.6 8.1 %copy-start.1 = (f32[128,1024]{1,0:T(8,128)S(1)}, f32[128,1024]{1,0:T(8,128)}, u32[]{:S(2)}) copy-start(f32[128,1024]{1,0:T(8,128)} %all-reduce.3.cloned.1.call-done) | copy-start | bytes 1572868
  162.6 68.2 %reduce-scatter.9.cloned.1.call-start = ((), (), s32[]{:S(2)}) async-start(), calls=%async_computation.7 | async-start | bytes 1802240 | tf_op jit(solution)/shard_map/reduce_scatter | solution.py:17
  170.4 129.5 %all-reduce.5.cloned.1.call-start = ((), (), s32[]{:S(2)}) async-start(), calls=%async_computation.9 | async-start | bytes 1048576 | tf_op jit(solution)/shard_map/psum | solution.py:32
  249.4 6.1 %copy-start.5 = (f32[1024]{0:T(1024)S(1)}, f32[1024]{0:T(1024)}, u32[]{:S(2)}) copy-start(f32[1024]{0:T(1024)} %param.29) | copy-start | bytes 12292
Sparse Core Ops, SparseCore 0:
  14.6 36.3 reduce-scatter.4
  53.3 32.1 reduce-scatter.6
  110.2 44.3 all-reduce.2
  162.7 33.6 reduce-scatter.10
  198.6 32.1 reduce-scatter.8
  255.6 44.3 all-reduce.4
where the time goes:
time: 309 us
  waiting for transfers between devices  183 us (59%)
  blocking collectives  60.5 us (20%)
  matrix products  43.4 us (14%)
  between operations  13.6 us (4%)
  other arithmetic  5 us (2%)
  local copies, waits for them, and re-layouts  3.12 us (1%)
    psum x2, waiting for transfers between devices, half_step(): branch = lax.psum(partial_value, 'cb')  88.9 us
    reduce_scatter x2, waiting for transfers between devices, half_step(): lax.psum_scatter(gate_part, 'ra', scatter_dimension=1, tiled=True)  47.4 us
    reduce_scatter x2, waiting for transfers between devices, half_step(): lax.psum_scatter(up_part, 'ra', scatter_dimension=1, tiled=True)  46.5 us
    all_gather x2, blocking collectives, half_step(): lax.all_gather(hidden, 'ra', axis=1, tiled=True)  34.4 us
    psum x2, blocking collectives, half_step(): total = lax.psum(squares, 'ra')  26.2 us
    dot_general x2, matrix products, half_step(): jnp.dot(scaled, up_w.astype(jnp.bfloat16), preferred_element_type=jnp.flo...  15.7 us
    dot_general x2, matrix products, half_step(): jnp.dot(scaled, gate_w.astype(jnp.bfloat16), preferred_element_type=jnp.f...  15.6 us
    dot_general x2, matrix products, half_step(): jnp.dot(lax.all_gather(hidden, 'ra', axis=1, tiled=True), down_bf, prefer...  12.1 us
  transfers between devices with their start and end apart: 6, of which 6 were waited for; matrix products, arithmetic and copies ran while one was open for 6% of the time, Pallas kernels for 0%

commit v1 on v0

v1 whole, which is shorter than its diff:
```python
import functools

import jax
import jax.numpy as jnp
from jax import lax
from jax.experimental import pallas as pl
from jax.experimental.pallas import tpu as pltpu
from jax.sharding import PartitionSpec as P

MESH = pl.DeviceIdType.MESH
F32 = jnp.float32
BF16 = jnp.bfloat16


def chunk_of(total):
    for size in (256, 128):
        if total % size == 0:
            return size
    return total


def kernel(
    nra,
    ncb,
    width,
    tokens_ref,
    gain1_ref,
    gscale1_ref,
    uscale1_ref,
    dscale1_ref,
    gain2_ref,
    gscale2_ref,
    uscale2_ref,
    dscale2_ref,
    gate1_hbm,
    up1_hbm,
    down1_hbm,
    gate2_hbm,
    up2_hbm,
    down2_hbm,
    out_ref,
    wg,
    wu,
    wd,
    stream,
    scaled,
    acc,
    squares,
    squares_in,
    part,
    part_in,
    hid,
    branch_part,
    branch_in,
    branch,
    wg_sem,
    wu_sem,
    wd_sem,
    part_send,
    part_recv,
    hid_send,
    hid_recv,
    small_send,
    small_recv,
):
    ra = lax.axis_index("ra")
    cb = lax.axis_index("cb")
    chunks, depth, size = wg.shape
    tokens = stream.shape[0]
    rows = tokens // nra
    crow = tokens // ncb

    def columns(c):
        return pl.ds(pl.multiple_of(c * size, size), size)

    def load_in(gate_hbm, up_hbm, c):
        return (
            pltpu.make_async_copy(gate_hbm.at[:, columns(c)], wg.at[c], wg_sem.at[c]),
            pltpu.make_async_copy(up_hbm.at[:, columns(c)], wu.at[c], wu_sem.at[c]),
        )

    def load_down(down_hbm, c):
        return pltpu.make_async_copy(down_hbm.at[columns(c), :], wd.at[c], wd_sem.at[c])

    def ra_peer(d):
        return lax.rem(ra + d, nra)

    def cb_peer(d):
        return lax.rem(cb + d, ncb)

    def wait_bytes(ref, sem):
        pltpu.make_async_copy(ref, ref, sem).wait()

    @pl.loop(0, chunks)
    def _(c):
        for copy in load_in(gate1_hbm, up1_hbm, c):
            copy.start()

    @pl.loop(0, chunks)
    def _(c):
        load_down(down1_hbm, c).start()

    barrier = pltpu.get_barrier_semaphore()
    for d in range(1, nra):
        pl.semaphore_signal(barrier, inc=1, device_id={"ra": ra_peer(d)}, device_id_type=MESH)
    for d in range(1, ncb):
        pl.semaphore_signal(barrier, inc=1, device_id={"cb": cb_peer(d)}, device_id_type=MESH)

    stream[...] = tokens_ref[...].astype(F32)
    pl.semaphore_wait(barrier, nra + ncb - 2)

    halves = (
        (gain1_ref, gscale1_ref, uscale1_ref, dscale1_ref, gate1_hbm, up1_hbm, down1_hbm),
        (gain2_ref, gscale2_ref, uscale2_ref, dscale2_ref, gate2_hbm, up2_hbm, down2_hbm),
    )
    for half in range(2):
        gain_ref, gscale_ref, uscale_ref, dscale_ref, gate_hbm, up_hbm, down_hbm = halves[half]
        value = stream[...]
        scaled[...] = (value * gain_ref[...]).astype(BF16)
        sums = jnp.sum(value * value, axis=1, keepdims=True)
        squares[...] = jnp.broadcast_to(sums, (tokens, 128)).reshape(nra, rows, 128)
        for d in range(1, nra):
            pltpu.make_async_remote_copy(
                src_ref=squares.at[ra_peer(d)],
                dst_ref=squares_in.at[d - 1],
                send_sem=small_send.at[0],
                recv_sem=small_recv.at[0],
                device_id={"ra": ra_peer(d)},
                device_id_type=MESH,
            ).start()

        @pl.loop(0, chunks)
        def _(c):
            for copy in load_in(gate_hbm, up_hbm, c):
                copy.wait()
            lhs = scaled[...]
            gate = jnp.dot(lhs, wg[c].astype(BF16), preferred_element_type=F32)
            up = jnp.dot(lhs, wu[c].astype(BF16), preferred_element_type=F32)
            part[c, :, :, :size] = gate.astype(BF16).reshape(nra, rows, size)
            part[c, :, :, size:] = up.astype(BF16).reshape(nra, rows, size)
            for d in range(1, nra):
                pltpu.make_async_remote_copy(
                    src_ref=part.at[c, ra_peer(d)],
                    dst_ref=part_in.at[c, d - 1],
                    send_sem=part_send.at[c],
                    recv_sem=part_recv.at[c],
                    device_id={"ra": ra_peer(d)},
                    device_id_type=MESH,
                ).start()
            if half == 0:
                for copy in load_in(gate2_hbm, up2_hbm, c):
                    copy.start()

        wait_bytes(squares_in, small_recv.at[0])
        total = squares[ra]
        for d in range(1, nra):
            total = total + squares_in[d - 1]
        squares_in[0] = lax.rsqrt(total / width + 1e-06)

        @pl.loop(0, chunks)
        def _(c):
            wait_bytes(part_in.at[c], part_recv.at[c])
            both = part[c, ra].astype(F32)
            for d in range(1, nra):
                both = both + part_in[c, d - 1].astype(F32)
            inverse = squares_in[0][:, :1]
            gate = both[:, :size] * inverse * gscale_ref[:, columns(c)]
            up = both[:, size:] * inverse * uscale_ref[:, columns(c)]
            hid[c, ra] = (gate / (1.0 + jnp.exp(-gate)) * up).astype(BF16)
            for d in range(1, nra):
                pltpu.make_async_remote_copy(
                    src_ref=hid.at[c, ra],
                    dst_ref=hid.at[c, ra],
                    send_sem=hid_send.at[c],
                    recv_sem=hid_recv.at[c],
                    device_id={"ra": ra_peer(d)},
                    device_id_type=MESH,
                ).start()

        acc[...] = jnp.zeros_like(acc)

        @pl.loop(0, chunks)
        def _(c):
            wait_bytes(hid.at[c, pl.ds(0, nra - 1)], hid_recv.at[c])
            load_down(down_hbm, c).wait()
            acc[...] += jnp.dot(
                hid[c].reshape(tokens, size), wd[c].astype(BF16), preferred_element_type=F32
            )
            if half == 0:
                load_down(down2_hbm, c).start()

        branch_part[...] = acc[...].astype(BF16).reshape(branch_part.shape)
        for d in range(1, ncb):
            pltpu.make_async_remote_copy(
                src_ref=branch_part.at[cb_peer(d)],
                dst_ref=branch_in.at[d - 1],
                send_sem=small_send.at[1],
                recv_sem=small_recv.at[1],
                device_id={"cb": cb_peer(d)},
                device_id_type=MESH,
            ).start()

        wait_bytes(squares_in, small_send.at[0])

        @pl.loop(0, chunks)
        def _(c):
            wait_bytes(part_in.at[c], part_send.at[c])
            wait_bytes(hid.at[c, pl.ds(0, nra - 1)], hid_send.at[c])

        wait_bytes(branch_in, small_recv.at[1])
        own = acc[pl.ds(pl.multiple_of(cb * crow, crow), crow), :]
        for d in range(1, ncb):
            own = own + branch_in[d - 1].astype(F32)
        branch[cb] = own.astype(BF16)
        for d in range(1, ncb):
            pltpu.make_async_remote_copy(
                src_ref=branch.at[cb],
                dst_ref=branch.at[cb],
                send_sem=small_send.at[2],
                recv_sem=small_recv.at[2],
                device_id={"cb": cb_peer(d)},
                device_id_type=MESH,
            ).start()
        wait_bytes(branch.at[pl.ds(0, ncb - 1)], small_recv.at[2])
        gathered = branch[...].reshape(tokens, depth).astype(F32)
        result = 0.5 * stream[...] + 0.5 * gathered * dscale_ref[...]
        if half == 0:
            stream[...] = result
        else:
            out_ref[...] = result
        wait_bytes(branch_in, small_send.at[1])
        wait_bytes(branch_in, small_send.at[2])


def local(nra, ncb, *args):
    (tokens, gain1, gate1, gscale1, up1, uscale1, down1, dscale1) = args[:8]
    (gain2, gate2, gscale2, up2, uscale2, down2, dscale2) = args[8:]
    count, depth = tokens.shape
    hidden = gate1.shape[1]
    size = chunk_of(hidden)
    chunks = hidden // size
    rows, crow = count // nra, count // ncb

    def row(vector):
        return vector.reshape(1, -1)

    vmem = pl.BlockSpec(memory_space=pltpu.VMEM)
    hbm = pl.BlockSpec(memory_space=pl.ANY)
    return pl.pallas_call(
        functools.partial(kernel, nra, ncb, float(depth * nra)),
        out_shape=jax.ShapeDtypeStruct((count, depth), F32),
        in_specs=[vmem] * 9 + [hbm] * 6,
        out_specs=vmem,
        scratch_shapes=[
            pltpu.VMEM((chunks, depth, size), F32),
            pltpu.VMEM((chunks, depth, size), F32),
            pltpu.VMEM((chunks, size, depth), F32),
            pltpu.VMEM((count, depth), F32),
            pltpu.VMEM((count, depth), BF16),
            pltpu.VMEM((count, depth), F32),
            pltpu.VMEM((nra, rows, 128), F32),
            pltpu.VMEM((nra - 1, rows, 128), F32),
            pltpu.VMEM((chunks, nra, rows, 2 * size), BF16),
            pltpu.VMEM((chunks, nra - 1, rows, 2 * size), BF16),
            pltpu.VMEM((chunks, nra, rows, size), BF16),
            pltpu.VMEM((ncb, crow, depth), BF16),
            pltpu.VMEM((ncb - 1, crow, depth), BF16),
            pltpu.VMEM((ncb, crow, depth), BF16),
            pltpu.SemaphoreType.DMA((chunks,)),
            pltpu.SemaphoreType.DMA((chunks,)),
            pltpu.SemaphoreType.DMA((chunks,)),
            pltpu.SemaphoreType.DMA((chunks,)),
            pltpu.SemaphoreType.DMA((chunks,)),
            pltpu.SemaphoreType.DMA((chunks,)),
            pltpu.SemaphoreType.DMA((chunks,)),
            pltpu.SemaphoreType.DMA((3,)),
            pltpu.SemaphoreType.DMA((3,)),
        ],
        compiler_params=pltpu.CompilerParams(
            collective_id=0, has_side_effects=True, vmem_limit_bytes=60 * 1024 * 1024
        ),
    )(
        tokens,
        row(gain1),
        row(gscale1),
        row(uscale1),
        row(dscale1),
        row(gain2),
        row(gscale2),
        row(uscale2),
        row(dscale2),
        gate1,
        up1,
        down1,
        gate2,
        up2,
        down2,
    )


def solution(mesh):
    half = (P("ra"), P("ra", "cb"), P("cb"), P("ra", "cb"), P("cb"), P("cb", "ra"), P("ra"))
    return jax.shard_map(
        functools.partial(local, mesh.shape["ra"], mesh.shape["cb"]),
        mesh=mesh,
        in_specs=(P("dp", "ra"),) + half + half,
        out_specs=P("dp", "ra"),
        check_vma=False,
    )
```

time: 309 us -> 130 us (0.42)
  waiting for transfers between devices: 183 us -> 0 us
  Pallas kernels: 0 us -> 123 us
  blocking collectives: 60.5 us -> 0 us
  matrix products: 43.4 us -> 0 us
  between operations: 13.6 us -> 0.01 us
  other arithmetic: 5 us -> 0 us
  local copies, waits for them, and re-layouts: 3.12 us -> 7.13 us
    pallas_call x0 -> x1, Pallas kernels: none -> 123 us  [local(): pl.pallas_call(functools.partial(kernel, nra, ncb, float(depth * nra)), o...]
    reduce_scatter x4 -> x0, waiting for transfers between devices: 93.9 us -> none  [the longest x2 47.4 us: half_step(): lax.psum_scatter(gate_part, 'ra', scatter_dimension=1, tiled=True)]
    psum x2 -> x0, waiting for transfers between devices: 88.9 us -> none  [half_step(): branch = lax.psum(partial_value, 'cb')]
    dot_general x6 -> x0, matrix products: 43.4 us -> none  [the longest x2 15.7 us: half_step(): jnp.dot(scaled, up_w.astype(jnp.bfloat16), preferred_element_type=jnp.flo...]
    all_gather x2 -> x0, blocking collectives: 34.4 us -> none  [half_step(): lax.all_gather(hidden, 'ra', axis=1, tiled=True)]
    psum x2 -> x0, blocking collectives: 26.2 us -> none  [half_step(): total = lax.psum(squares, 'ra')]
    reshape x0 -> x4, local copies, waits for them, and re-layouts: none -> 5.24 us  [row(): return vector.reshape(1, -1)]
    dynamic_slice x4 -> x0, local copies, waits for them, and re-layouts: 3.1 us -> none  [the longest x2 1.56 us: half_step(): gate_own = lax.dynamic_slice_in_dim(gate_scale, offset, columns, 0)]
  transfers between devices with their start and end apart: 6 -> 0, of which waited for: 6 -> 0; matrix products, arithmetic and copies ran while one was open for 6% -> 0% of each run, Pallas kernels for 0% -> 0%
where the time goes in v1:
time: 130 us
  Pallas kernels  123 us (95%)
  local copies, waits for them, and re-layouts  7.13 us (5%)
    pallas_call x1, Pallas kernels, local(): pl.pallas_call(functools.partial(kernel, nra, ncb, float(depth * nra)), o...  123 us
    reshape x4, local copies, waits for them, and re-layouts, row(): return vector.reshape(1, -1)  5.24 us

profile of v1, /device:TPU:0, one launch (start us, length us, event | category | flops | bytes accessed | tf_op | source)
XLA Modules:
  0.0 129.7 jit_solution(8884614751266932784)
XLA Ops:
  0.0 1.3 %reshape.25.gscale1_ref = f32[1,2816]{1,0:T(1,128)} reshape(f32[2816]{0:T(1024)} %param.18) | data formatting | bytes 22528 | tf_op jit(solution)/shard_map/reshape | solution.py:245
  1.3 1.3 %reshape.26.uscale1_ref = f32[1,2816]{1,0:T(1,128)} reshape(f32[2816]{0:T(1024)} %param.20) | data formatting | bytes 22528 | tf_op jit(solution)/shard_map/reshape | solution.py:245
  2.6 1.3 %reshape.29.gscale2_ref = f32[1,2816]{1,0:T(1,128)} reshape(f32[2816]{0:T(1024)} %param.25) | data formatting | bytes 22528 | tf_op jit(solution)/shard_map/reshape | solution.py:245
  3.9 1.3 %reshape.30.uscale2_ref = f32[1,2816]{1,0:T(1,128)} reshape(f32[2816]{0:T(1024)} %param.27) | data formatting | bytes 22528 | tf_op jit(solution)/shard_map/reshape | solution.py:245
  5.2 122.6 %shard_map.145 = f32[128,1024]{1,0:T(8,128)} custom-call(bf16[128,1024]{1,0:T(8,128)(2,1)} %tokens_ref.1, f32[1,1024]{1,0:T(1,128)} %bitcast.4, f32[1,2816]{1,0:T(1,128)} %reshape.25.gscale1_ref, f32[1,2816]{1,0:T(1,128)} %reshape.26.uscale1_ref, f32[1,1024]{1,0:T(1,128)} %bitcast.5, f32[1,1024]{1,0:T(1,128)} %bitcast.6, f32[1,2816]{1,0:T(1,128)} %reshape.29.gscale2_ref, ...), custom_call_target="tpu_custom_call" | custom-call | tf_op jit(solution)/shard_map/pallas_call | solution.py:249
  127.8 1.9 %copy.17 = f32[128,1024]{1,0:T(8,128)} copy(f32[128,1024]{1,0:T(8,128)} %shard_map.145) | data formatting | bytes 1048576

commit v2 on v1

--- a/solution.py
+++ b/solution.py
@@ -10,6 +10,8 @@
 MESH = pl.DeviceIdType.MESH
 F32 = jnp.float32
 BF16 = jnp.bfloat16
+REDUCE_LAG = 3
+GATHER_LAG = 3
 
 
 def chunk_of(total):
@@ -47,7 +49,9 @@
     acc,
     squares,
     squares_in,
+    inverse_ref,
     part,
+    part_out,
     part_in,
     hid,
     branch_part,
@@ -60,6 +64,7 @@
     part_recv,
     hid_send,
     hid_recv,
+    squares_send,
     small_send,
     small_recv,
 ):
@@ -67,8 +72,9 @@
     cb = lax.axis_index("cb")
     chunks, depth, size = wg.shape
     tokens = stream.shape[0]
-    rows = tokens // nra
+    rows = tokens // 2
     crow = tokens // ncb
+    last = nra - 1
 
     def columns(c):
         return pl.ds(pl.multiple_of(c * size, size), size)
@@ -82,14 +88,16 @@
     def load_down(down_hbm, c):
         return pltpu.make_async_copy(down_hbm.at[columns(c), :], wd.at[c], wd_sem.at[c])
 
-    def ra_peer(d):
-        return lax.rem(ra + d, nra)
-
     def cb_peer(d):
         return lax.rem(cb + d, ncb)
 
     def wait_bytes(ref, sem):
         pltpu.make_async_copy(ref, ref, sem).wait()
+
+    hops = (last - ra, ra)
+    onward = (lax.rem(ra + nra - 1, nra), lax.rem(ra + 1, nra))
+    back = (onward[1], onward[0])
+    owner = (0, last)
 
     @pl.loop(0, chunks)
     def _(c):
@@ -102,7 +110,8 @@
 
     barrier = pltpu.get_barrier_semaphore()
     for d in range(1, nra):
-        pl.semaphore_signal(barrier, inc=1, device_id={"ra": ra_peer(d)}, device_id_type=MESH)
+        peer = lax.rem(ra + d, nra)
+        pl.semaphore_signal(barrier, inc=1, device_id={"ra": peer}, device_id_type=MESH)
     for d in range(1, ncb):
         pl.semaphore_signal(barrier, inc=1, device_id={"cb": cb_peer(d)}, device_id_type=MESH)
 
@@ -118,76 +127,121 @@
         value = stream[...]
         scaled[...] = (value * gain_ref[...]).astype(BF16)
         sums = jnp.sum(value * value, axis=1, keepdims=True)
-        squares[...] = jnp.broadcast_to(sums, (tokens, 128)).reshape(nra, rows, 128)
-        for d in range(1, nra):
-            pltpu.make_async_remote_copy(
-                src_ref=squares.at[ra_peer(d)],
-                dst_ref=squares_in.at[d - 1],
-                send_sem=small_send.at[0],
-                recv_sem=small_recv.at[0],
-                device_id={"ra": ra_peer(d)},
-                device_id_type=MESH,
-            ).start()
-
-        @pl.loop(0, chunks)
-        def _(c):
-            for copy in load_in(gate_hbm, up_hbm, c):
-                copy.wait()
-            lhs = scaled[...]
-            gate = jnp.dot(lhs, wg[c].astype(BF16), preferred_element_type=F32)
-            up = jnp.dot(lhs, wu[c].astype(BF16), preferred_element_type=F32)
-            part[c, :, :, :size] = gate.astype(BF16).reshape(nra, rows, size)
-            part[c, :, :, size:] = up.astype(BF16).reshape(nra, rows, size)
-            for d in range(1, nra):
+        squares[...] = jnp.broadcast_to(sums, (tokens, 128)).reshape(2, rows, 128)
+        for f in range(2):
+            @pl.when(hops[f] < last)
+            def _(f=f):
                 pltpu.make_async_remote_copy(
-                    src_ref=part.at[c, ra_peer(d)],
-                    dst_ref=part_in.at[c, d - 1],
-                    send_sem=part_send.at[c],
-                    recv_sem=part_recv.at[c],
-                    device_id={"ra": ra_peer(d)},
+                    src_ref=squares.at[f],
+                    dst_ref=squares_in.at[hops[f]],
+                    send_sem=squares_send.at[f],
+                    recv_sem=small_recv.at[0],
+                    device_id={"ra": owner[f]},
                     device_id_type=MESH,
                 ).start()
-            if half == 0:
-                for copy in load_in(gate2_hbm, up2_hbm, c):
-                    copy.start()
-
-        wait_bytes(squares_in, small_recv.at[0])
-        total = squares[ra]
-        for d in range(1, nra):
-            total = total + squares_in[d - 1]
-        squares_in[0] = lax.rsqrt(total / width + 1e-06)
-
-        @pl.loop(0, chunks)
-        def _(c):
-            wait_bytes(part_in.at[c], part_recv.at[c])
-            both = part[c, ra].astype(F32)
-            for d in range(1, nra):
-                both = both + part_in[c, d - 1].astype(F32)
-            inverse = squares_in[0][:, :1]
-            gate = both[:, :size] * inverse * gscale_ref[:, columns(c)]
-            up = both[:, size:] * inverse * uscale_ref[:, columns(c)]
-            hid[c, ra] = (gate / (1.0 + jnp.exp(-gate)) * up).astype(BF16)
-            for d in range(1, nra):
-                pltpu.make_async_remote_copy(
-                    src_ref=hid.at[c, ra],
-                    dst_ref=hid.at[c, ra],
-                    send_sem=hid_send.at[c],
-                    recv_sem=hid_recv.at[c],
-                    device_id={"ra": ra_peer(d)},
-                    device_id_type=MESH,
-                ).start()
 
         acc[...] = jnp.zeros_like(acc)
 
-        @pl.loop(0, chunks)
-        def _(c):
-            wait_bytes(hid.at[c, pl.ds(0, nra - 1)], hid_recv.at[c])
-            load_down(down_hbm, c).wait()
-            acc[...] += jnp.dot(
-                hid[c].reshape(tokens, size), wd[c].astype(BF16), preferred_element_type=F32
+        def reduce_step(f, c):
+            send = pltpu.make_async_remote_copy(
+                src_ref=part_out.at[f, c],
+                dst_ref=part_in.at[f, c],
+                send_sem=part_send.at[f, c],
+                recv_sem=part_recv.at[f, c],
+                device_id={"ra": onward[f]},
+                device_id_type=MESH,
             )
-            if half == 0:
-                load_down(down2_hbm, c).start()
+
+            @pl.when(hops[f] == 0)
+            def _():
+                part_out[f, c] = part[c, f].astype(BF16)
+                send.start()
+
+            @pl.when(jnp.logical_and(hops[f] > 0, hops[f] < last))
+            def _():
+                wait_bytes(part_in.at[f, c], part_recv.at[f, c])
+                part_out[f, c] = (part[c, f] + part_in[f, c].astype(F32)).astype(BF16)
+                send.start()
+
+            @pl.when(hops[f] == last)
+            def _():
+                @pl.when(c == 0)
+                def _():
+                    wait_bytes(squares_in, small_recv.at[0])
+                    total = squares[f]
+                    for d in range(last):
+                        total = total + squares_in[d]
+                    inverse_ref[...] = lax.rsqrt(total / width + 1e-06)
+
+                wait_bytes(part_in.at[f, c], part_recv.at[f, c])
+                both = part[c, f] + part_in[f, c].astype(F32)
+                inverse = inverse_ref[:, :1]
+                gate = both[:, :size] * inverse * gscale_ref[:, columns(c)]
+                up = both[:, size:] * inverse * uscale_ref[:, columns(c)]
+                hid[c, f] = (gate / (1.0 + jnp.exp(-gate)) * up).astype(BF16)
+                forward(f, c).start()
+
+        def forward(f, c):
+            return pltpu.make_async_remote_copy(
+                src_ref=hid.at[c, f],
+                dst_ref=hid.at[c, f],
+                send_sem=hid_send.at[f, c],
+                recv_sem=hid_recv.at[f, c],
+                device_id={"ra": back[f]},
+                device_id_type=MESH,
+            )
+
+        def gather_step(f, c):
+            @pl.when(hops[f] < last)
+            def _():
+                wait_bytes(hid.at[c, f], hid_recv.at[f, c])
+
+                @pl.when(hops[f] > 0)
+                def _():
+                    forward(f, c).start()
+
+        def at_lag(step, lag, act):
+            c = step - lag
+
+            @pl.when(jnp.logical_and(c >= 0, c < chunks))
+            def _():
+                act(c)
+
+        @pl.loop(0, chunks + (REDUCE_LAG + GATHER_LAG) * last)
+        def _(step):
+            @pl.when(step < chunks)
+            def _():
+                c = step
+                for copy in load_in(gate_hbm, up_hbm, c):
+                    copy.wait()
+                lhs = scaled[...]
+                gate = jnp.dot(lhs, wg[c].astype(BF16), preferred_element_type=F32)
+                up = jnp.dot(lhs, wu[c].astype(BF16), preferred_element_type=F32)
+                part[c, :, :, :size] = gate.reshape(2, rows, size)
+                part[c, :, :, size:] = up.reshape(2, rows, size)
+                if half == 0:
+                    for copy in load_in(gate2_hbm, up2_hbm, c):
+                        copy.start()
+
+            for f in range(2):
+                at_lag(step, REDUCE_LAG * hops[f], functools.partial(reduce_step, f))
+            for f in range(2):
+                at_lag(
+                    step,
+                    REDUCE_LAG * last + GATHER_LAG * (last - hops[f]),
+                    functools.partial(gather_step, f),
+                )
+
+            def down_step(c):
+                load_down(down_hbm, c).wait()
+                acc[...] += jnp.dot(
+                    hid[c].reshape(tokens, size), wd[c].astype(BF16), preferred_element_type=F32
+                )
+                if half == 0:
+                    load_down(down2_hbm, c).start()
+
+            nearest = jnp.minimum(hops[0], hops[1])
+            at_lag(step, REDUCE_LAG * last + GATHER_LAG * (last - nearest), down_step)
 
         branch_part[...] = acc[...].astype(BF16).reshape(branch_part.shape)
         for d in range(1, ncb):
@@ -200,12 +254,20 @@
                 device_id_type=MESH,
             ).start()
 
-        wait_bytes(squares_in, small_send.at[0])
-
-        @pl.loop(0, chunks)
-        def _(c):
-            wait_bytes(part_in.at[c], part_send.at[c])
-            wait_bytes(hid.at[c, pl.ds(0, nra - 1)], hid_send.at[c])
+        for f in range(2):
+            @pl.when(hops[f] < last)
+            def _(f=f):
+                wait_bytes(squares.at[f], squares_send.at[f])
+
+                @pl.loop(0, chunks)
+                def _(c):
+                    wait_bytes(part_out.at[f, c], part_send.at[f, c])
+
+            @pl.when(hops[f] > 0)
+            def _(f=f):
+                @pl.loop(0, chunks)
+                def _(c):
+                    wait_bytes(hid.at[c, f], hid_send.at[f, c])
 
         wait_bytes(branch_in, small_recv.at[1])
         own = acc[pl.ds(pl.multiple_of(cb * crow, crow), crow), :]
@@ -239,7 +301,7 @@
     hidden = gate1.shape[1]
     size = chunk_of(hidden)
     chunks = hidden // size
-    rows, crow = count // nra, count // ncb
+    rows, crow = count // 2, count // ncb
 
     def row(vector):
         return vector.reshape(1, -1)
@@ -258,21 +320,24 @@
             pltpu.VMEM((count, depth), F32),
             pltpu.VMEM((count, depth), BF16),
             pltpu.VMEM((count, depth), F32),
-            pltpu.VMEM((nra, rows, 128), F32),
+            pltpu.VMEM((2, rows, 128), F32),
             pltpu.VMEM((nra - 1, rows, 128), F32),
-            pltpu.VMEM((chunks, nra, rows, 2 * size), BF16),
-            pltpu.VMEM((chunks, nra - 1, rows, 2 * size), BF16),
-            pltpu.VMEM((chunks, nra, rows, size), BF16),
+            pltpu.VMEM((rows, 128), F32),
+            pltpu.VMEM((chunks, 2, rows, 2 * size), F32),
+            pltpu.VMEM((2, chunks, rows, 2 * size), BF16),
+            pltpu.VMEM((2, chunks, rows, 2 * size), BF16),
+            pltpu.VMEM((chunks, 2, rows, size), BF16),
             pltpu.VMEM((ncb, crow, depth), BF16),
             pltpu.VMEM((ncb - 1, crow, depth), BF16),
             pltpu.VMEM((ncb, crow, depth), BF16),
             pltpu.SemaphoreType.DMA((chunks,)),
             pltpu.SemaphoreType.DMA((chunks,)),
             pltpu.SemaphoreType.DMA((chunks,)),
-            pltpu.SemaphoreType.DMA((chunks,)),
-            pltpu.SemaphoreType.DMA((chunks,)),
-            pltpu.SemaphoreType.DMA((chunks,)),
-            pltpu.SemaphoreType.DMA((chunks,)),
+            pltpu.SemaphoreType.DMA((2, chunks)),
+            pltpu.SemaphoreType.DMA((2, chunks)),
+            pltpu.SemaphoreType.DMA((2, chunks)),
+            pltpu.SemaphoreType.DMA((2, chunks)),
+            pltpu.SemaphoreType.DMA((2,)),
             pltpu.SemaphoreType.DMA((3,)),
             pltpu.SemaphoreType.DMA((3,)),
         ],

time: 130 us -> 104 us (0.80)
  Pallas kernels: 123 us -> 96 us
    pallas_call x1, Pallas kernels: 123 us -> 96 us  [local(): pl.pallas_call(functools.partial(kernel, nra, ncb, float(depth * nra)), o...]
where the time goes in v2:
time: 104 us; the launch traced here: 103 us
  Pallas kernels  96 us (92%)
  local copies, waits for them, and re-layouts  7.13 us (7%)
    pallas_call x1, Pallas kernels, local(): pl.pallas_call(functools.partial(kernel, nra, ncb, float(depth * nra)), o...  96 us
    reshape x4, local copies, waits for them, and re-layouts, row(): return vector.reshape(1, -1)  5.24 us

profile of v2, /device:TPU:0, one launch (start us, length us, event | category | flops | bytes accessed | tf_op | source)
XLA Modules:
  0.0 103.2 jit_solution(9000074808441518632)
XLA Ops:
  0.0 1.3 %reshape.25.gscale1_ref = f32[1,2816]{1,0:T(1,128)} reshape(f32[2816]{0:T(1024)} %param.18) | data formatting | bytes 22528 | tf_op jit(solution)/shard_map/reshape | solution.py:307
  1.3 1.3 %reshape.26.uscale1_ref = f32[1,2816]{1,0:T(1,128)} reshape(f32[2816]{0:T(1024)} %param.20) | data formatting | bytes 22528 | tf_op jit(solution)/shard_map/reshape | solution.py:307
  2.6 1.3 %reshape.29.gscale2_ref = f32[1,2816]{1,0:T(1,128)} reshape(f32[2816]{0:T(1024)} %param.25) | data formatting | bytes 22528 | tf_op jit(solution)/shard_map/reshape | solution.py:307
  3.9 1.3 %reshape.30.uscale2_ref = f32[1,2816]{1,0:T(1,128)} reshape(f32[2816]{0:T(1024)} %param.27) | data formatting | bytes 22528 | tf_op jit(solution)/shard_map/reshape | solution.py:307
  5.2 96.0 %shard_map.145 = f32[128,1024]{1,0:T(8,128)} custom-call(bf16[128,1024]{1,0:T(8,128)(2,1)} %tokens_ref.1, f32[1,1024]{1,0:T(1,128)} %bitcast.4, f32[1,2816]{1,0:T(1,128)} %reshape.25.gscale1_ref, f32[1,2816]{1,0:T(1,128)} %reshape.26.uscale1_ref, f32[1,1024]{1,0:T(1,128)} %bitcast.5, f32[1,1024]{1,0:T(1,128)} %bitcast.6, f32[1,2816]{1,0:T(1,128)} %reshape.29.gscale2_ref, ...), custom_call_target="tpu_custom_call" | custom-call | tf_op jit(solution)/shard_map/pallas_call | solution.py:311
  101.3 1.9 %copy.17 = f32[128,1024]{1,0:T(8,128)} copy(f32[128,1024]{1,0:T(8,128)} %shard_map.145) | data formatting | bytes 1048576
